TPU v7x, 32 devices: a whole 2x2x4 slice. The times are simulated.
32 devices in a mesh: grp: 2 (over y), sp: 4 (over z), tp: 4 (over x, core).
Axes of the slice: x: 2, y: 2, z: 4, core: 2. Of those that a mesh axis runs over, the one named last changes fastest.
Arguments:
- queries_small: bfloat16 [2048, 1024], P(('grp', 'sp'), 'tp'), parts along dimension 0, may hold values from -6 to 6
- keys_small: bfloat16 [2048, 512], P(('grp', 'sp'), 'tp'), parts along dimension 0, may hold values from -6 to 6
- values_small: bfloat16 [2048, 512], P(('grp', 'sp'), 'tp'), parts along dimension 0, may hold values from -6 to 6
- queries_large: bfloat16 [2048, 1024], P(('grp', 'sp'), 'tp'), parts along dimension 0, may hold values from -6 to 6
- keys_large: bfloat16 [2048, 512], P(('grp', 'sp'), 'tp'), parts along dimension 0, may hold values from -6 to 6
- values_large: bfloat16 [2048, 512], P(('grp', 'sp'), 'tp'), parts along dimension 0, may hold values from -6 to 6
- query_gain_small: float32 [128], P('grp'), parts along dimension 0, may hold values from 1.2 to 12
- key_gain_small: float32 [128], P('grp'), parts along dimension 0, may hold values from 1.2 to 12
- query_gain_large: float32 [256], P('grp'), parts along dimension 0, may hold values from 1.2 to 12
- key_gain_large: float32 [256], P('grp'), parts along dimension 0, may hold values from 1.2 to 12
- residual_in: bfloat16 [2048, 2048], P(('grp', 'sp', 'tp')), parts along dimension 0, may hold values from -1.5 to 1.5
- out_weight_small: bfloat16 [1024, 2048], P('tp'), may hold values from -0.125 to 0.125
- out_weight_large: bfloat16 [1024, 2048], P('tp'), may hold values from -0.125 to 0.125
- norm_gain: float32 [2048], replicated, may hold values from 0.1 to 1.9
- routes: int32 [2048, 2], P(('grp', 'sp', 'tp')), parts along dimension 0, may hold values from 0 to 7, all different within a row; in each aligned block of 64 rows (0 to 63, 64 to 127, ...) at most 32 rows name the same one
- route_scores: float32 [2048, 2], P(('grp', 'sp', 'tp')), parts along dimension 0, may hold values from 0.05 to 1
- expert_gate: bfloat16 [8, 2048, 1024], P('sp', None, 'tp'), may hold values from -0.125 to 0.125
- expert_up: bfloat16 [8, 2048, 1024], P('sp', None, 'tp'), may hold values from -0.125 to 0.125
- expert_down: bfloat16 [8, 1024, 2048], P('sp', 'tp'), may hold values from -0.1875 to 0.1875
Outputs:
- result: bfloat16 [2048, 2048], P(('grp', 'sp', 'tp')), parts along dimension 0
There are 2 independent parts, one for each index of `grp`. A program takes and returns all parts, laid end to end along the dimension named above; an argument that names none is the same for every part. Nothing has to cross between parts.
Inputs may be any that keep to these rules, and one draw needn't show every extreme that they name: `routes`: each token names 2 different experts; within the rows of one device (aligned blocks of 64 tokens) no expert is named more than 32 times, a bound that some block reaches.
All inputs are finite; a program needn't handle non-finite values.
Results may differ from a plain program's by a relative error of at most 0.02.
The roundings to bfloat16 on the way count: a program that leaves them out, or rounds other values in their place, can miss the bound.
Values may be sent and summed in bfloat16 or wider, within the bound.
A program may use at most 128 MiB of HBM per device.

v0:
```python
import jax
import jax.numpy as jnp
from jax import lax
from jax.sharding import PartitionSpec as P

HS_SMALL = 64
HS_LARGE = 128
GRID_W = 64
theta_base = 10000.0
norm_eps = 1e-06
block_target = 1280


def grid_tables(offset, length, head_size):
    places = offset + jnp.arange(length, dtype=jnp.int32)
    grid_rows = (places // GRID_W).astype(jnp.float32)
    grid_cols = (places % GRID_W).astype(jnp.float32)
    rates = jnp.power(
        theta_base, -2.0 * jnp.arange(head_size // 4, dtype=jnp.float32) / (head_size // 2)
    )
    row_angles = grid_rows[:, None, None] * rates
    col_angles = grid_cols[:, None, None] * rates
    return (jnp.cos(row_angles), jnp.sin(row_angles), jnp.cos(col_angles), jnp.sin(col_angles))


def half_turn(segment, cosine, sine_part):
    half_size = segment.shape[-1] // 2
    leading = segment[..., :half_size]
    trailing = segment[..., half_size:]
    return jnp.concatenate(
        [leading * cosine - trailing * sine_part, trailing * cosine + leading * sine_part], axis=-1
    )


def grid_turn(vectors, tables):
    row_cos, row_sin, col_cos, col_sin = tables
    half_size = vectors.shape[-1] // 2
    return jnp.concatenate(
        [
            half_turn(vectors[..., :half_size], row_cos, row_sin),
            half_turn(vectors[..., half_size:], col_cos, col_sin),
        ],
        axis=-1,
    )


def normed_turn(raw_rows, gain, tables):
    widened = raw_rows.astype(jnp.float32)
    scaled = (
        widened * lax.rsqrt(jnp.mean(widened * widened, axis=-1, keepdims=True) + norm_eps) * gain
    )
    return grid_turn(scaled, tables).astype(jnp.bfloat16)


def block_rows(row_count, shard_rows):
    shards = row_count // shard_rows
    chosen = 1
    for factor in range(1, max(1, block_target // shard_rows) + 1):
        if shards % factor == 0:
            chosen = factor
    return chosen * shard_rows


def attend_block(state, queries, key_rows, value_rows):
    largest, weight_sum, accumulated = state
    head_size = queries.shape[-1]
    kv_local = queries.shape[1]
    key_heads = key_rows.reshape(key_rows.shape[0], kv_local, head_size)
    value_heads = value_rows.reshape(value_rows.shape[0], kv_local, head_size)
    scores = jnp.einsum(
        "qgrd,kgd->qgrk", queries, key_heads, preferred_element_type=jnp.float32
    ) * head_size ** (-0.5)
    peak_score = jnp.maximum(largest, jnp.max(scores, axis=-1))
    shrink = jnp.exp(largest - peak_score)
    weights = jnp.exp(scores - peak_score[..., None])
    weight_sum = weight_sum * shrink + jnp.sum(weights, axis=-1)
    accumulated = accumulated * shrink[..., None] + jnp.einsum(
        "qgrk,kgd->qgrd",
        weights.astype(jnp.bfloat16),
        value_heads,
        preferred_element_type=jnp.float32,
    )
    return (peak_score, weight_sum, accumulated)


def attend_rows(state, queries, key_rows, value_rows):
    row_count = key_rows.shape[0]
    step_rows = block_rows(row_count, queries.shape[0])
    if step_rows == row_count:
        return attend_block(state, queries, key_rows, value_rows)

    def one_block(block_index, carried):
        offset = block_index * step_rows
        return attend_block(
            carried,
            queries,
            lax.dynamic_slice_in_dim(key_rows, offset, step_rows, 0),
            lax.dynamic_slice_in_dim(value_rows, offset, step_rows, 0),
        )

    return lax.fori_loop(0, row_count // step_rows, one_block, state)


def empty_state(queries):
    state_shape = queries.shape[:3]
    return (
        jnp.full(state_shape, -1e30, jnp.float32),
        jnp.zeros(state_shape, jnp.float32),
        jnp.zeros(queries.shape, jnp.float32),
    )


def finish(state):
    largest, weight_sum, accumulated = state
    merged = accumulated / weight_sum[..., None]
    return merged.reshape(merged.shape[0], -1).astype(jnp.bfloat16)


def on_device(
    queries_small,
    keys_small,
    values_small,
    queries_large,
    keys_large,
    values_large,
    query_gain_small,
    key_gain_small,
    query_gain_large,
    key_gain_large,
    residual_in,
    out_weight_small,
    out_weight_large,
    norm_gain,
    routes,
    route_scores,
    expert_gate,
    expert_up,
    expert_down,
):
    token_rows = queries_small.shape[0]
    offset = lax.axis_index("sp") * token_rows
    tables_small = grid_tables(offset, token_rows, HS_SMALL)
    tables_large = grid_tables(offset, token_rows, HS_LARGE)
    kv_small = keys_small.shape[1] // HS_SMALL
    kv_large = keys_large.shape[1] // HS_LARGE
    asked_small = normed_turn(
        queries_small.reshape(token_rows, -1, HS_SMALL), query_gain_small, tables_small
    ).reshape(token_rows, kv_small, -1, HS_SMALL)
    asked_large = normed_turn(
        queries_large.reshape(token_rows, -1, HS_LARGE), query_gain_large, tables_large
    ).reshape(token_rows, kv_large, -1, HS_LARGE)
    turned_small = normed_turn(
        keys_small.reshape(token_rows, kv_small, HS_SMALL), key_gain_small, tables_small
    ).reshape(token_rows, -1)
    turned_large = normed_turn(
        keys_large.reshape(token_rows, kv_large, HS_LARGE), key_gain_large, tables_large
    ).reshape(token_rows, -1)
    key_small = lax.all_gather(turned_small, "sp", axis=0, tiled=True)
    value_small = lax.all_gather(values_small, "sp", axis=0, tiled=True)
    key_large = lax.all_gather(turned_large, "sp", axis=0, tiled=True)
    value_large = lax.all_gather(values_large, "sp", axis=0, tiled=True)
    state_small = attend_rows(empty_state(asked_small), asked_small, key_small, value_small)
    state_large = attend_rows(empty_state(asked_large), asked_large, key_large, value_large)
    heard_small = finish(state_small)
    heard_large = finish(state_large)
    projected = lax.psum_scatter(
        (
            jnp.dot(heard_small, out_weight_small, preferred_element_type=jnp.float32)
            + jnp.dot(heard_large, out_weight_large, preferred_element_type=jnp.float32)
        ).astype(jnp.bfloat16),
        "tp",
        scatter_dimension=0,
        tiled=True,
    ).astype(jnp.float32)
    attended = (residual_in.astype(jnp.float32) + projected).astype(jnp.bfloat16)
    widened = attended.astype(jnp.float32)
    normed = (
        widened
        * lax.rsqrt(jnp.mean(widened * widened, axis=-1, keepdims=True) + norm_eps)
        * norm_gain
    ).astype(jnp.bfloat16)
    local_rows = routes.shape[0]
    top_count = routes.shape[1]
    sp_count = lax.axis_size("sp")
    local_experts = expert_gate.shape[0]
    expert_count = local_experts * sp_count
    capacity = max(2, (2 * top_count * local_rows + expert_count - 1) // expert_count)
    flat_routes = routes.reshape(-1)
    member = (flat_routes[:, None] == jnp.arange(expert_count, dtype=jnp.int32)[None, :]).astype(
        jnp.int32
    )
    ranks = jnp.sum((jnp.cumsum(member, axis=0) - member) * member, axis=1)
    slots = flat_routes * capacity + ranks
    picker = (
        slots[:, None] == jnp.arange(expert_count * capacity, dtype=jnp.int32)[None, :]
    ).astype(jnp.bfloat16)
    placer = jnp.sum(picker.reshape(local_rows, top_count, -1), axis=1)
    outgoing = jnp.einsum("ts,td->sd", placer, normed, preferred_element_type=jnp.float32).astype(
        jnp.bfloat16
    )
    outgoing = outgoing.reshape(sp_count, local_experts, capacity, -1)
    everyone = lax.all_gather(
        lax.all_to_all(outgoing, "sp", split_axis=0, concat_axis=0, tiled=True),
        "tp",
        axis=0,
        tiled=True,
    )
    gate_out = jnp.einsum(
        "secd,edf->secf", everyone, expert_gate, preferred_element_type=jnp.float32
    )
    up_out = jnp.einsum("secd,edf->secf", everyone, expert_up, preferred_element_type=jnp.float32)
    active = (jax.nn.silu(gate_out) * up_out).astype(jnp.bfloat16)
    summed = lax.psum_scatter(
        jnp.einsum(
            "secf,efd->secd", active, expert_down, preferred_element_type=jnp.float32
        ).astype(jnp.bfloat16),
        "tp",
        scatter_dimension=0,
        tiled=True,
    )
    returned = lax.all_to_all(summed, "sp", split_axis=0, concat_axis=0, tiled=True)
    back_rows = returned.reshape(expert_count * capacity, -1)
    chosen_rows = jnp.dot(picker, back_rows, preferred_element_type=jnp.float32).reshape(
        local_rows, top_count, -1
    )
    shares = route_scores / jnp.sum(route_scores, axis=1, keepdims=True)
    mixed = jnp.sum(chosen_rows * shares[:, :, None], axis=1)
    return (attended.astype(jnp.float32) + mixed).astype(jnp.bfloat16)


def solution(mesh):
    in_specs = (
        P(("grp", "sp"), "tp"),
        P(("grp", "sp"), "tp"),
        P(("grp", "sp"), "tp"),
        P(("grp", "sp"), "tp"),
        P(("grp", "sp"), "tp"),
        P(("grp", "sp"), "tp"),
        P("grp"),
        P("grp"),
        P("grp"),
        P("grp"),
        P(("grp", "sp", "tp"), None),
        P("tp", None),
        P("tp", None),
        P(),
        P(("grp", "sp", "tp"), None),
        P(("grp", "sp", "tp"), None),
        P("sp", None, "tp"),
        P("sp", None, "tp"),
        P("sp", "tp", None),
    )
    out_specs = P(("grp", "sp", "tp"), None)
    return jax.shard_map(
        on_device, mesh=mesh, in_specs=in_specs, out_specs=out_specs, check_vma=False
    )
```

profile of v0, /device:TPU:0, one launch (start us, length us, event | category | flops | bytes accessed | tf_op | source)
XLA Modules:
  0.0 313.0 jit_solution(7394251430156797041)
XLA Ops:
  6.6 1.1 copy.83
  7.7 0.7 fusion.63
  8.5 1.0 multiply_cosine_fusion.1
  9.8 15.7 %all_gather.17 = bf16[1024,128]{0,1:T(8,128)(2,1)S(1)} all-gather(bf16[256,128]{0,1:T(8,128)(2,1)S(1)} %pad_maximum_fusion.1), channel_id=1, replica_groups=mesh['grp'=2,'sp'=4,'tp'=4] {'sp'}, dimensions={0}, use_global_device_ids=true | all-gather | bytes 327680 | tf_op jit(solution)/shard_map/all_gather | solution.py:160
  25.5 1.0 copy.84
  27.1 0.6 bitcast_reduce_fusion.1
  27.8 1.3 copy-done.2
  29.5 14.4 %all_gather.18 = bf16[1024,128]{0,1:T(8,128)(2,1)S(1)} all-gather(bf16[256,128]{0,1:T(8,128)(2,1)S(1)} %copy.87), channel_id=1, replica_groups=mesh['grp'=2,'sp'=4,'tp'=4] {'sp'}, dimensions={0}, use_global_device_ids=true | all-gather | bytes 327680 | tf_op jit(solution)/shard_map/all_gather | solution.py:161
  44.5 13.8 %all_gather.15 = bf16[1024,128]{0,1:T(8,128)(2,1)S(1)} all-gather(bf16[256,128]{0,1:T(8,128)(2,1)S(1)} %bitcast.168), channel_id=1, replica_groups=mesh['grp'=2,'sp'=4,'tp'=4] {'sp'}, dimensions={0}, use_global_device_ids=true | all-gather | bytes 327680 | tf_op jit(solution)/shard_map/all_gather | solution.py:158
  58.6 0.8 bitcast_reduce_fusion
  59.4 0.7 fusion.1
  60.1 1.2 copy-done.1
  61.3 13.8 %all_gather.16 = bf16[1024,128]{1,0:T(8,128)(2,1)S(1)} all-gather(bf16[256,128]{1,0:T(8,128)(2,1)S(1)} %copy-done.8), channel_id=1, replica_groups=mesh['grp'=2,'sp'=4,'tp'=4] {'sp'}, dimensions={0}, use_global_device_ids=true | all-gather | bytes 327680 | tf_op jit(solution)/shard_map/all_gather | solution.py:159
  75.3 3.1 fusion.38
  78.9 1.1 copy-done.3
  80.5 1.5 fusion.3
  83.1 25.4 %reduce-scatter.5.cloned.1.call-done = bf16[64,2048]{1,0:T(8,128)(2,1)} async-done(((bf16[256,2048]{1,0:T(8,128)(2,1)}), bf16[64,2048]{1,0:T(8,128)(2,1)}) %reduce-scatter.5.cloned.1.call-update) | async-done | bytes 262160 | tf_op jit(solution)/shard_map/reduce_scatter | solution.py:166
  108.5 1.1 fusion.48
  109.7 1.4 convolution_convert_fusion
  111.1 30.0 %all_to_all.10 = bf16[4,2,32,2048]{3,2,1,0:T(8,128)(2,1)S(1)} all-to-all(bf16[4,2,32,2048]{3,2,1,0:T(8,128)(2,1)S(1)} %bitcast.163), channel_id=1, replica_groups=mesh['grp'=2,'sp'=4,'tp'=4] {'sp'}, dimensions={0} | all-to-all | bytes 2097152 | tf_op jit(solution)/shard_map/all_to_all | solution.py:203
  141.1 1.0 copy.91
  142.4 32.5 %all-gather.2.cloned.1.call-done = bf16[16,2,32,2048]{3,2,0,1:T(8,128)(2,1)} async-done(((bf16[4,2,32,2048]{3,2,0,1:T(8,128)(2,1)}), bf16[16,2,32,2048]{3,2,0,1:T(8,128)(2,1)}) %all-gather.2.cloned.1.call-update) | async-done | bytes 4194320 | tf_op jit(solution)/shard_map/all_gather | solution.py:202
  174.9 4.1 %fusion.14 = f32[16,2,32,256]{3,2,0,1:T(8,128)S(1)} fusion(bf16[16,2,32,2048]{3,2,0,1:T(8,128)(2,1)} %all-gather.2.cloned.1.call-done, bf16[2,2048,256]{2,1,0:T(8,128)(2,1)} %param.35), kind=kOutput, calls=%fused_computation.21 | convolution fusion | flops 1073741824 | bytes 7340032 | tf_op jit(solution)/shard_map/secd,edf->secf/dot_general | solution.py:208
  179.0 7.3 %convert_bitcast_fusion = bf16[16,2,32,2048]{3,2,0,1:T(8,128)(2,1)} fusion(bf16[2,256,2048]{2,1,0:T(8,128)(2,1)S(1)} %copy-done, bf16[16,2,32,2048]{3,2,0,1:T(8,128)(2,1)} %all-gather.2.cloned.1.call-done, bf16[2,2048,256]{2,1,0:T(8,128)(2,1)} %param.36, f32[16,2,32,256]{3,2,0,1:T(8,128)S(1)} %fusion.14), kind=kOutput, calls=%fused_computation.3 | convolution fusion | flops 2151153664 | bytes 13631488 | tf_op jit(solution)/shard_map/secf,efd->secd/dot_general | solution.py:214
  186.3 0.6 copy-done.17
  187.0 0.6 dynamic-slice
  188.2 83.8 %all-reduce.3.cloned.1.call-done = bf16[16,2,32,2048]{3,2,0,1:T(8,128)(2,1)} async-done(((bf16[16,2,32,2048]{3,2,0,1:T(8,128)(2,1)}), bf16[16,2,32,2048]{3,2,0,1:T(8,128)(2,1)}) %all-reduce.3.cloned.1.call-update) | async-done | bytes 4194320
  272.0 1.3 constant_dynamic-slice_fusion
  273.3 1.1 copy.92
  274.4 4.6 %all-to-all-start.1 = ((bf16[4,2,32,2048]{3,2,1,0:T(8,128)(2,1)}), bf16[4,2,32,2048]{3,2,1,0:T(8,128)(2,1)S(1)}, u32[]{:S(2)}, u32[]{:S(2)}) async-start(bf16[4,2,32,2048]{3,2,1,0:T(8,128)(2,1)} %copy.92), calls=%async_computation.2 | async-start | bytes 2097152 | tf_op jit(solution)/shard_map/all_to_all | solution.py:221
  279.0 25.4 %all-to-all-done.1 = bf16[4,2,32,2048]{3,2,1,0:T(8,128)(2,1)S(1)} async-done(((bf16[4,2,32,2048]{3,2,1,0:T(8,128)(2,1)}), bf16[4,2,32,2048]{3,2,1,0:T(8,128)(2,1)S(1)}, u32[]{:S(2)}, u32[]{:S(2)}) %all-to-all-start.1) | async-done | bytes 1048608 | tf_op jit(solution)/shard_map/all_to_all | solution.py:221
  304.7 1.7 fusion.51
  (84 shorter events, 5.1 us)
Async XLA Ops:
  6.5 172.5 %copy-start = (bf16[2,256,2048]{2,1,0:T(8,128)(2,1)S(1)}, bf16[2,256,2048]{2,1,0:T(8,128)(2,1)}, u32[]{:S(2)}) copy-start(bf16[2,256,2048]{2,1,0:T(8,128)(2,1)} %param.37) | copy-start | bytes 6291460
  6.5 20.1 %copy-start.14 = (f32[128]{0:T(128)S(1)}, f32[128]{0:T(128)}, u32[]{:S(2)}) copy-start(f32[128]{0:T(128)} %param.27) | copy-start | bytes 1540
  6.5 102.0 %reduce-scatter.5.cloned.1.call-start = ((), (), s32[]{:S(2)}) async-start(), calls=%async_computation.3 | async-start | bytes 1310720 | tf_op jit(solution)/shard_map/reduce_scatter | solution.py:166
  27.1 2.4 copy-start.9
  27.1 17.1 %copy-start.10 = (bf16[256,128]{1,0:T(8,128)(2,1)S(1)}, bf16[256,128]{1,0:T(8,128)(2,1)}, u32[]{:S(2)}) copy-start(bf16[256,128]{1,0:T(8,128)(2,1)} %param.20) | copy-start | bytes 196612
  27.7 1.3 copy-start.2
  27.7 16.6 %copy-start.15 = (f32[64]{0:T(128)S(1)}, f32[64]{0:T(128)}, u32[]{:S(2)}) copy-start(f32[64]{0:T(128)} %param.26) | copy-start | bytes 772
  27.7 30.6 %copy-start.7 = (bf16[256,256]{1,0:T(8,128)(2,1)S(1)}, bf16[256,256]{1,0:T(8,128)(2,1)}, u32[]{:S(2)}) copy-start(bf16[256,256]{1,0:T(8,128)(2,1)} %param.19) | copy-start | bytes 393220
  27.7 30.7 %copy-start.16 = (f32[64]{0:T(128)S(1)}, f32[64]{0:T(128)}, u32[]{:S(2)}) copy-start(f32[64]{0:T(128)} %param.25) | copy-start | bytes 772
  59.4 1.9 copy-start.1
  59.4 1.9 copy-start.8
  75.3 3.1 copy-start.5
  78.4 1.6 copy-start.3
  78.9 1.6 copy-start.6
  80.5 1.6 copy-start.12
  80.5 28.0 %copy-start.4 = (bf16[64,2048]{1,0:T(8,128)(2,1)S(1)}, bf16[64,2048]{1,0:T(8,128)(2,1)}, u32[]{:S(2)}) copy-start(bf16[64,2048]{1,0:T(8,128)(2,1)} %param.29) | copy-start | bytes 786436
  80.5 29.1 %copy-start.11 = (f32[2048]{0:T(1024)S(1)}, f32[2048]{0:T(1024)}, u32[]{:S(2)}) copy-start(f32[2048]{0:T(1024)} %param.32) | copy-start | bytes 24580
  82.0 92.9 %all-gather.2.cloned.1.call-start = ((), (), s32[]{:S(2)}) async-start(), calls=%async_computation.4 | async-start | bytes 5242880 | tf_op jit(solution)/shard_map/all_gather | solution.py:202
  142.1 129.9 %all-reduce.3.cloned.1.call-start = ((), (), s32[]{:S(2)}) async-start(), calls=%async_computation.5 | async-start | bytes 8388608
  186.3 0.7 copy-start.17
  273.3 5.7 %copy-start.13 = (f32[64,2]{0,1:T(2,128)S(1)}, f32[64,2]{0,1:T(2,128)}, u32[]{:S(2)}) copy-start(f32[64,2]{0,1:T(2,128)} %param.34) | copy-start | bytes 1540
  274.4 30.0 %all-to-all-start.1 = ((bf16[4,2,32,2048]{3,2,1,0:T(8,128)(2,1)}), bf16[4,2,32,2048]{3,2,1,0:T(8,128)(2,1)S(1)}, u32[]{:S(2)}, u32[]{:S(2)}) async-start(bf16[4,2,32,2048]{3,2,1,0:T(8,128)(2,1)} %copy.92), calls=%async_computation.2 | async-start | bytes 2097152 | tf_op jit(solution)/shard_map/all_to_all | solution.py:221
Sparse Core Ops, SparseCore 0:
  82.1 26.3 reduce-scatter.4
  142.3 32.5 all-gather.1
  186.5 85.4 all-reduce.2
where the time goes:
time: 313 us
  waiting for transfers between devices  167 us (53%)
  blocking collectives  87.7 us (28%)
  matrix products  20.1 us (6%)
  between operations  14.3 us (5%)
  local copies, waits for them, and re-layouts  11.3 us (4%)
  other arithmetic  7.66 us (2%)
  starting transfers between devices  4.86 us (2%)
    unnamed x4, waiting for transfers between devices  83.8 us
    all_gather x1, waiting for transfers between devices, on_device(): lax.all_gather(lax.all_to_all(outgoing, 'sp', split_axis=0, concat_axis=0...  32.5 us
    all_to_all x1, blocking collectives, on_device(): lax.all_to_all(outgoing, 'sp', split_axis=0, concat_axis=0, tiled=True)  30 us
    reduce_scatter x1, waiting for transfers between devices, on_device(): lax.psum_scatter((jnp.dot(heard_small, out_weight_small, preferred_elemen...  25.4 us
    all_to_all x1, waiting for transfers between devices, on_device(): lax.all_to_all(summed, 'sp', split_axis=0, concat_axis=0, tiled=True)  25.4 us
    all_gather x1, blocking collectives, on_device(): key_large = lax.all_gather(turned_large, 'sp', axis=0, tiled=True)  15.7 us
    all_gather x1, blocking collectives, on_device(): value_large = lax.all_gather(values_large, 'sp', axis=0, tiled=True)  14.4 us
    all_gather x1, blocking collectives, on_device(): key_small = lax.all_gather(turned_small, 'sp', axis=0, tiled=True)  13.8 us
  transfers between devices with their start and end apart: 4, of which 4 were waited for; matrix products, arithmetic and copies ran while one was open for 1% of the time, Pallas kernels for 0%

commit v1 on v0

--- a/solution.py
+++ b/solution.py
@@ -156,8 +156,13 @@
         keys_large.reshape(token_rows, kv_large, HS_LARGE), key_gain_large, tables_large
     ).reshape(token_rows, -1)
     key_small = lax.all_gather(turned_small, "sp", axis=0, tiled=True)
-    value_small = lax.all_gather(values_small, "sp", axis=0, tiled=True)
-    key_large = lax.all_gather(turned_large, "sp", axis=0, tiled=True)
+    value_small, key_large = jnp.split(
+        lax.all_gather(
+            jnp.concatenate([values_small, turned_large], axis=1), "sp", axis=0, tiled=True
+        ),
+        [values_small.shape[1]],
+        axis=1,
+    )
     value_large = lax.all_gather(values_large, "sp", axis=0, tiled=True)
     state_small = attend_rows(empty_state(asked_small), asked_small, key_small, value_small)
     state_large = attend_rows(empty_state(asked_large), asked_large, key_large, value_large)

time: 313 us -> 303 us (0.968)
  blocking collectives: 87.7 us -> 75.8 us
    all_gather x2 -> x1, blocking collectives: 29.4 us -> 17.4 us  [on_device(): lax.all_gather(jnp.concatenate([values_small, turned_large], axis=1), 'sp...]
    unnamed x44 -> x46, local copies, waits for them, and re-layouts: 8.64 us -> 8.67 us
where the time goes in v1:
time: 303 us
  waiting for transfers between devices  167 us (55%)
  blocking collectives  75.8 us (25%)
  matrix products  20.1 us (7%)
  between operations  14.3 us (5%)
  local copies, waits for them, and re-layouts  12.8 us (4%)
  other arithmetic  8.17 us (3%)
  starting transfers between devices  4.86 us (2%)
    unnamed x4, waiting for transfers between devices  83.8 us
    all_gather x1, waiting for transfers between devices, on_device(): lax.all_gather(lax.all_to_all(outgoing, 'sp', split_axis=0, concat_axis=0...  32.5 us
    all_to_all x1, blocking collectives, on_device(): lax.all_to_all(outgoing, 'sp', split_axis=0, concat_axis=0, tiled=True)  29.9 us
    all_to_all x1, waiting for transfers between devices, on_device(): lax.all_to_all(summed, 'sp', split_axis=0, concat_axis=0, tiled=True)  25.4 us
    reduce_scatter x1, waiting for transfers between devices, on_device(): lax.psum_scatter((jnp.dot(heard_small, out_weight_small, preferred_elemen...  25.2 us
    all_gather x1, blocking collectives, on_device(): lax.all_gather(jnp.concatenate([values_small, turned_large], axis=1), 'sp...  17.4 us
    all_gather x1, blocking collectives, on_device(): value_large = lax.all_gather(values_large, 'sp', axis=0, tiled=True)  14.7 us
    all_gather x1, blocking collectives, on_device(): key_small = lax.all_gather(turned_small, 'sp', axis=0, tiled=True)  13.8 us
  transfers between devices with their start and end apart: 4, of which 4 were waited for; matrix products, arithmetic and copies ran while one was open for 1% of the time, Pallas kernels for 0%

profile of v1, /device:TPU:0, one launch (start us, length us, event | category | flops | bytes accessed | tf_op | source)
XLA Modules:
  0.0 302.9 jit_solution(11383160169731471180)
XLA Ops:
  7.1 1.0 copy.81
  8.1 0.7 fusion.62
  8.9 1.0 multiply_cosine_fusion.1
  10.7 1.0 concatenate.50
  11.7 17.4 %all_gather.13 = bf16[1024,256]{1,0:T(8,128)(2,1)S(1)} all-gather(bf16[256,256]{1,0:T(8,128)(2,1)S(1)} %concatenate.50), channel_id=1, replica_groups=mesh['grp'=2,'sp'=4,'tp'=4] {'sp'}, dimensions={0}, use_global_device_ids=true | all-gather | bytes 655360 | tf_op jit(solution)/shard_map/all_gather | solution.py:160
  29.0 1.1 copy.88
  30.8 0.6 bitcast_reduce_fusion.1
  31.5 1.3 copy-done.2
  33.2 14.7 %all_gather.14 = bf16[1024,128]{0,1:T(8,128)(2,1)S(1)} all-gather(bf16[256,128]{0,1:T(8,128)(2,1)S(1)} %copy.90), channel_id=1, replica_groups=mesh['grp'=2,'sp'=4,'tp'=4] {'sp'}, dimensions={0}, use_global_device_ids=true | all-gather | bytes 327680 | tf_op jit(solution)/shard_map/all_gather | solution.py:166
  48.5 13.8 %all_gather.12 = bf16[1024,128]{0,1:T(8,128)(2,1)S(1)} all-gather(bf16[256,128]{0,1:T(8,128)(2,1)S(1)} %bitcast.168), channel_id=1, replica_groups=mesh['grp'=2,'sp'=4,'tp'=4] {'sp'}, dimensions={0}, use_global_device_ids=true | all-gather | bytes 327680 | tf_op jit(solution)/shard_map/all_gather | solution.py:158
  62.6 0.8 bitcast_reduce_fusion
  63.4 0.7 fusion.1
  64.1 1.2 copy-done.1
  65.5 3.1 %fusion.38 = bf16[256,2,2,64]{0,3,2,1:T(8,128)(2,1)S(1)} fusion(bf16[1024,2,64,1]{0,2,3,1:T(8,128)(2,1)S(1)} %bitcast.166, f32[2,1024,256,2]{2,1,3,0:T(8,128)} %copy-done.1, f32[256,2,2]{0,2,1:T(2,128)S(1)} %broadcast_maximum_fusion, f32[256,2,2]{0,2,1:T(2,128)S(1)} %get-tuple-element.30, f32[256,2,2]{0,2,1:T(2,128)S(1)} %get-tuple-element.29), kind=kOutput, calls=%fused_computation.32 | convolution fusion | flops 137560064 | bytes 4599808 | tf_op jit(solution)/shard_map/qgrk,kgd->qgrd/dot_general | solution.py:77
  69.1 1.1 copy-done.3
  70.7 1.5 fusion.3
  73.3 25.2 %reduce-scatter.5.cloned.1.call-done = bf16[64,2048]{1,0:T(8,128)(2,1)} async-done(((bf16[256,2048]{1,0:T(8,128)(2,1)}), bf16[64,2048]{1,0:T(8,128)(2,1)}) %reduce-scatter.5.cloned.1.call-update) | async-done | bytes 262160 | tf_op jit(solution)/shard_map/reduce_scatter | solution.py:171
  98.5 1.1 fusion.48
  99.6 1.4 convolution_convert_fusion
  101.1 29.9 %all_to_all.10 = bf16[4,2,32,2048]{3,2,1,0:T(8,128)(2,1)S(1)} all-to-all(bf16[4,2,32,2048]{3,2,1,0:T(8,128)(2,1)S(1)} %bitcast.163), channel_id=1, replica_groups=mesh['grp'=2,'sp'=4,'tp'=4] {'sp'}, dimensions={0} | all-to-all | bytes 2097152 | tf_op jit(solution)/shard_map/all_to_all | solution.py:208
  131.0 1.0 copy.94
  132.3 32.5 %all-gather.2.cloned.1.call-done = bf16[16,2,32,2048]{3,2,0,1:T(8,128)(2,1)} async-done(((bf16[4,2,32,2048]{3,2,0,1:T(8,128)(2,1)}), bf16[16,2,32,2048]{3,2,0,1:T(8,128)(2,1)}) %all-gather.2.cloned.1.call-update) | async-done | bytes 4194320 | tf_op jit(solution)/shard_map/all_gather | solution.py:207
  164.8 4.1 %fusion.14 = f32[16,2,32,256]{3,2,0,1:T(8,128)S(1)} fusion(bf16[16,2,32,2048]{3,2,0,1:T(8,128)(2,1)} %all-gather.2.cloned.1.call-done, bf16[2,2048,256]{2,1,0:T(8,128)(2,1)} %param.35), kind=kOutput, calls=%fused_computation.21 | convolution fusion | flops 1073741824 | bytes 7340032 | tf_op jit(solution)/shard_map/secd,edf->secf/dot_general | solution.py:213
  169.0 7.3 %convert_bitcast_fusion = bf16[16,2,32,2048]{3,2,0,1:T(8,128)(2,1)} fusion(bf16[2,256,2048]{2,1,0:T(8,128)(2,1)S(1)} %copy-done, bf16[16,2,32,2048]{3,2,0,1:T(8,128)(2,1)} %all-gather.2.cloned.1.call-done, bf16[2,2048,256]{2,1,0:T(8,128)(2,1)} %param.36, f32[16,2,32,256]{3,2,0,1:T(8,128)S(1)} %fusion.14), kind=kOutput, calls=%fused_computation.3 | convolution fusion | flops 2151153664 | bytes 13631488 | tf_op jit(solution)/shard_map/secf,efd->secd/dot_general | solution.py:219
  176.3 0.6 copy-done.18
  176.9 0.6 dynamic-slice
  178.2 83.8 %all-reduce.3.cloned.1.call-done = bf16[16,2,32,2048]{3,2,0,1:T(8,128)(2,1)} async-done(((bf16[16,2,32,2048]{3,2,0,1:T(8,128)(2,1)}), bf16[16,2,32,2048]{3,2,0,1:T(8,128)(2,1)}) %all-reduce.3.cloned.1.call-update) | async-done | bytes 4194320
  261.9 1.3 constant_dynamic-slice_fusion
  263.3 1.1 copy.95
  264.3 4.6 %all-to-all-start.1 = ((bf16[4,2,32,2048]{3,2,1,0:T(8,128)(2,1)}), bf16[4,2,32,2048]{3,2,1,0:T(8,128)(2,1)S(1)}, u32[]{:S(2)}, u32[]{:S(2)}) async-start(bf16[4,2,32,2048]{3,2,1,0:T(8,128)(2,1)} %copy.95), calls=%async_computation.2 | async-start | bytes 2097152 | tf_op jit(solution)/shard_map/all_to_all | solution.py:226
  268.9 25.4 %all-to-all-done.1 = bf16[4,2,32,2048]{3,2,1,0:T(8,128)(2,1)S(1)} async-done(((bf16[4,2,32,2048]{3,2,1,0:T(8,128)(2,1)}), bf16[4,2,32,2048]{3,2,1,0:T(8,128)(2,1)S(1)}, u32[]{:S(2)}, u32[]{:S(2)}) %all-to-all-start.1) | async-done | bytes 1048608 | tf_op jit(solution)/shard_map/all_to_all | solution.py:226
  294.7 1.7 fusion.51
  (91 shorter events, 6.1 us)
Async XLA Ops:
  6.5 162.4 %copy-start = (bf16[2,256,2048]{2,1,0:T(8,128)(2,1)S(1)}, bf16[2,256,2048]{2,1,0:T(8,128)(2,1)}, u32[]{:S(2)}) copy-start(bf16[2,256,2048]{2,1,0:T(8,128)(2,1)} %param.37) | copy-start | bytes 6291460
  6.5 23.8 %copy-start.14 = (f32[128]{0:T(128)S(1)}, f32[128]{0:T(128)}, u32[]{:S(2)}) copy-start(f32[128]{0:T(128)} %param.27) | copy-start | bytes 1540
  6.5 91.9 %reduce-scatter.5.cloned.1.call-start = ((), (), s32[]{:S(2)}) async-start(), calls=%async_computation.3 | async-start | bytes 1310720 | tf_op jit(solution)/shard_map/reduce_scatter | solution.py:171
  29.0 2.4 copy-start.5
  30.8 2.4 copy-start.9
  30.8 17.2 %copy-start.17 = (f32[16]{0:T(128)S(1)}, f32[16]{0:T(128)}, u32[]{:S(2)}) copy-start(f32[16]{0:T(128)} %multiply_power_fusion.1) | copy-start | bytes 196
  30.8 17.4 %copy-start.10 = (bf16[256,128]{1,0:T(8,128)(2,1)S(1)}, bf16[256,128]{1,0:T(8,128)(2,1)}, u32[]{:S(2)}) copy-start(bf16[256,128]{1,0:T(8,128)(2,1)} %param.20) | copy-start | bytes 196612
  31.4 1.3 copy-start.2
  31.4 16.9 %copy-start.15 = (f32[64]{0:T(128)S(1)}, f32[64]{0:T(128)}, u32[]{:S(2)}) copy-start(f32[64]{0:T(128)} %param.26) | copy-start | bytes 772
  31.4 30.8 %copy-start.8 = (bf16[256,256]{1,0:T(8,128)(2,1)S(1)}, bf16[256,256]{1,0:T(8,128)(2,1)}, u32[]{:S(2)}) copy-start(bf16[256,256]{1,0:T(8,128)(2,1)} %param.19) | copy-start | bytes 393220
  31.5 31.0 %copy-start.16 = (f32[64]{0:T(128)S(1)}, f32[64]{0:T(128)}, u32[]{:S(2)}) copy-start(f32[64]{0:T(128)} %param.25) | copy-start | bytes 772
  63.4 1.9 copy-start.1
  63.4 1.9 slice-start
  65.5 3.1 %copy-start.6 = (bf16[256,2048]{1,0:T(8,128)(2,1)S(1)}, bf16[256,2048]{1,0:T(8,128)(2,1)}, u32[]{:S(2)}) copy-start(bf16[256,2048]{1,0:T(8,128)(2,1)} %param.30) | copy-start | bytes 3145732
  68.6 1.6 copy-start.3
  69.0 1.6 copy-start.7
  70.7 1.6 copy-start.12
  70.7 27.8 %copy-start.4 = (bf16[64,2048]{1,0:T(8,128)(2,1)S(1)}, bf16[64,2048]{1,0:T(8,128)(2,1)}, u32[]{:S(2)}) copy-start(bf16[64,2048]{1,0:T(8,128)(2,1)} %param.29) | copy-start | bytes 786436
  70.7 28.9 %copy-start.11 = (f32[2048]{0:T(1024)S(1)}, f32[2048]{0:T(1024)}, u32[]{:S(2)}) copy-start(f32[2048]{0:T(1024)} %param.32) | copy-start | bytes 24580
  72.2 92.6 %all-gather.2.cloned.1.call-start = ((), (), s32[]{:S(2)}) async-start(), calls=%async_computation.4 | async-start | bytes 5242880 | tf_op jit(solution)/shard_map/all_gather | solution.py:207
  132.1 129.9 %all-reduce.3.cloned.1.call-start = ((), (), s32[]{:S(2)}) async-start(), calls=%async_computation.5 | async-start | bytes 8388608
  176.3 0.7 copy-start.18
  263.2 5.7 %copy-start.13 = (f32[64,2]{0,1:T(2,128)S(1)}, f32[64,2]{0,1:T(2,128)}, u32[]{:S(2)}) copy-start(f32[64,2]{0,1:T(2,128)} %param.34) | copy-start | bytes 1540
  264.3 30.0 %all-to-all-start.1 = ((bf16[4,2,32,2048]{3,2,1,0:T(8,128)(2,1)}), bf16[4,2,32,2048]{3,2,1,0:T(8,128)(2,1)S(1)}, u32[]{:S(2)}, u32[]{:S(2)}) async-start(bf16[4,2,32,2048]{3,2,1,0:T(8,128)(2,1)} %copy.95), calls=%async_computation.2 | async-start | bytes 2097152 | tf_op jit(solution)/shard_map/all_to_all | solution.py:226
Sparse Core Ops, SparseCore 0:
  72.3 26.0 reduce-scatter.4
  132.2 32.5 all-gather.1
  176.4 85.4 all-reduce.2
